TPU v7x, 32 devices: a whole 2x2x4 slice. The times are simulated.
32 devices in a mesh: ep: 8 (over z, x), tp: 4 (over y, core).
Axes of the slice: x: 2, y: 2, z: 4, core: 2. Of those that a mesh axis runs over, the one named last changes fastest.
Arguments:
- residual: bfloat16 [256, 2048], P('ep'), may hold values from -6 to 6
- routes: int32 [256, 4], P('ep'), may hold values from 0 to 7, as said below
- lengths: int32 [256], P('ep'), may hold values from 1 to 512, as said below
- key_cache: bfloat16 [256, 512, 4, 128], P('ep', None, 'tp'), may hold values from -6 to 6
- value_cache: bfloat16 [256, 512, 4, 128], P('ep', None, 'tp'), may hold values from -6 to 6
- mix_gain: float32 [2048], replicated, may hold values from 0.1 to 1.9
- w_query: bfloat16 [2048, 2048], P(None, 'tp'), may hold values from -0.125 to 0.125
- w_out: bfloat16 [2048, 2048], P('tp'), may hold values from -0.375 to 0.375
- head_bias: float32 [16], P('tp'), may hold values from -7 to -1
- moe_gain: float32 [2048], replicated, may hold values from 0.1 to 1.9
- w_group: bfloat16 [2048, 1], replicated, may hold values from -0.02734375 to 0.02734375
- w_expert: bfloat16 [2048, 8], replicated, may hold values from -0.02734375 to 0.02734375
- expert_gate: bfloat16 [8, 2048, 1024], P('ep', None, 'tp'), may hold values from -0.125 to 0.125
- expert_up: bfloat16 [8, 2048, 1024], P('ep', None, 'tp'), may hold values from -0.125 to 0.125
- expert_down: bfloat16 [8, 1024, 2048], P('ep', 'tp'), may hold values from -3 to 3
Outputs:
- layer_out: bfloat16 [256, 2048], P('ep', 'tp')
Inputs may be any that keep to these rules, and one draw needn't show every extreme that they name: `routes`: each row names 4 different experts, all in one group of 8 consecutive experts. Within the rows of one device (aligned blocks of 32 rows) no expert is named more than 16 times, and some expert is named exactly 16 times in every block. `lengths`: some sequence has 512 cached positions in every draw.
All inputs are finite; a program needn't handle non-finite values.
Results may differ from a plain program's by a relative error of at most 0.02.
Values may be sent and summed in bfloat16 or wider, within the bound.
A program may use at most 64 MiB of HBM per device.

v0:
```python
import jax
import jax.numpy as jnp
from jax import lax
from jax.sharding import PartitionSpec as P

GROUP_SIZE = 8
TOPK = 4
EPSILON = 1e-06


def rms_scale(tokens, gains):
    values = tokens.astype(jnp.float32)
    inverse = lax.rsqrt(jnp.mean(values * values, axis=-1, keepdims=True) + EPSILON)
    return (values * inverse * gains).astype(jnp.bfloat16)


def stick_read(queries, key_rows, value_rows, head_bias, lengths):
    seq_count = queries.shape[0]
    key_heads = key_rows.shape[2]
    head_size = key_rows.shape[3]
    per_key = head_bias.shape[0] // key_heads
    grouped = queries.reshape(seq_count, key_heads, per_key, head_size)
    scores = jnp.einsum(
        "tkgd,tlkd->tkgl", grouped, key_rows, preferred_element_type=jnp.float32
    ) * head_size ** (-0.5)
    scores = scores + head_bias.reshape(1, key_heads, per_key, 1)
    inside = lax.broadcasted_iota(jnp.int32, scores.shape, 3) < lengths[:, None, None, None]
    remain = jnp.where(inside, jax.nn.log_sigmoid(-scores), 0.0)
    later_sum = lax.cumsum(remain, axis=3, reverse=True) - remain
    weights = jnp.where(inside, jnp.exp(jax.nn.log_sigmoid(scores) + later_sum), 0.0).astype(
        jnp.bfloat16
    )
    mixture = jnp.einsum("tkgl,tlkd->tkgd", weights, value_rows, preferred_element_type=jnp.float32)
    return mixture.astype(jnp.bfloat16).reshape(seq_count, key_heads * per_key * head_size)


def per_device(
    residual,
    routes,
    lengths,
    key_cache,
    value_cache,
    mix_gain,
    w_query,
    w_out,
    head_bias,
    moe_gain,
    w_group,
    w_expert,
    expert_gate,
    expert_up,
    expert_down,
):
    seq_count = residual.shape[0]
    width = residual.shape[1]
    own_width = width // lax.axis_size("tp")
    own_start = lax.axis_index("tp") * own_width
    normed = rms_scale(residual, mix_gain)
    queries = jnp.dot(normed, w_query, preferred_element_type=jnp.float32).astype(jnp.bfloat16)
    attended = stick_read(queries, key_cache, value_cache, head_bias, lengths)
    head_part = (
        jnp.dot(attended, w_out, preferred_element_type=jnp.float32)
        .astype(jnp.bfloat16)
        .astype(jnp.float32)
    )
    attn_own = lax.psum_scatter(
        head_part.astype(jnp.bfloat16), "tp", scatter_dimension=1, tiled=True
    )
    res_own = lax.dynamic_slice_in_dim(residual, own_start, own_width, 1)
    mid_own = (res_own.astype(jnp.float32) + attn_own.astype(jnp.float32)).astype(jnp.bfloat16)
    mid_values = mid_own.astype(jnp.float32)
    squares = lax.psum(jnp.sum(mid_values * mid_values, axis=1), "tp")
    inverse = lax.rsqrt(squares / width + EPSILON)
    gain_own = lax.dynamic_slice_in_dim(moe_gain, own_start, own_width, 0)
    send_rows = (mid_values * inverse[:, None] * gain_own[None, :]).astype(jnp.bfloat16)
    hidden_in = lax.all_gather(send_rows, "tp", axis=1, tiled=True)
    expert_count = w_expert.shape[1]
    group_count = w_group.shape[1]
    group_prob = jax.nn.softmax(
        jnp.dot(hidden_in, w_group, preferred_element_type=jnp.float32), axis=-1
    )
    expert_logit = jnp.dot(hidden_in, w_expert, preferred_element_type=jnp.float32)
    expert_ids = jnp.arange(expert_count, dtype=jnp.int32)
    chosen = routes[:, :, None] == expert_ids[None, None, :]
    picked = jnp.sum(jnp.where(chosen, expert_logit[:, None, :], 0.0), axis=2)
    group_hot = routes[:, :1] // GROUP_SIZE == jnp.arange(group_count, dtype=jnp.int32)[None, :]
    top_prob = jnp.sum(jnp.where(group_hot, group_prob, 0.0), axis=1, keepdims=True)
    share = jax.nn.softmax(picked, axis=1) * top_prob
    group_most = min(seq_count, max(4, 2 * seq_count // group_count))
    capacity = group_most * TOPK // GROUP_SIZE
    flat_hot = chosen.reshape(seq_count * TOPK, expert_count).astype(jnp.int32)
    earlier = jnp.cumsum(flat_hot, axis=0, dtype=jnp.int32) - flat_hot
    slot = jnp.sum(earlier * flat_hot, axis=1, dtype=jnp.int32)
    target = routes.reshape(-1) * capacity + slot
    placing = target[:, None] == jnp.arange(expert_count * capacity, dtype=jnp.int32)[None, :]
    placing = placing.reshape(seq_count, TOPK, expert_count * capacity)
    token_place = jnp.sum(placing.astype(jnp.int32), axis=1).astype(jnp.bfloat16)
    outgoing = jnp.einsum("sq,sd->qd", token_place, send_rows, preferred_element_type=jnp.float32)
    outgoing = outgoing.astype(jnp.bfloat16).reshape(expert_count, capacity, send_rows.shape[1])
    local_experts = expert_gate.shape[0]
    arrived = lax.all_to_all(outgoing, "ep", split_axis=0, concat_axis=0, tiled=True)
    arrived = lax.all_gather(arrived, "tp", axis=2, tiled=True)
    sources = arrived.shape[0] // local_experts
    batch_rows = arrived.reshape(sources, local_experts, arrived.shape[1], arrived.shape[2])
    gate = jnp.einsum("nxcd,xdf->nxcf", batch_rows, expert_gate, preferred_element_type=jnp.float32)
    upward = jnp.einsum("nxcd,xdf->nxcf", batch_rows, expert_up, preferred_element_type=jnp.float32)
    active = (jax.nn.silu(gate) * upward).astype(jnp.bfloat16)
    partial_value = jnp.einsum(
        "nxcf,xfd->nxcd", active, expert_down, preferred_element_type=jnp.float32
    )
    partial_value = partial_value.astype(jnp.bfloat16).astype(jnp.float32)
    partial_value = partial_value.reshape(
        arrived.shape[0], arrived.shape[1], partial_value.shape[3]
    )
    summed = lax.psum_scatter(
        partial_value.astype(jnp.bfloat16), "tp", scatter_dimension=2, tiled=True
    )
    returned = lax.all_to_all(summed, "ep", split_axis=0, concat_axis=0, tiled=True)
    combine = jnp.einsum(
        "sk,skq->sq", share, placing.astype(jnp.float32), precision=lax.Precision.HIGHEST
    )
    moe = jnp.dot(
        combine,
        returned.reshape(expert_count * capacity, own_width).astype(jnp.float32),
        precision=lax.Precision.HIGHEST,
    )
    return (mid_own.astype(jnp.float32) + moe).astype(jnp.bfloat16)


def solution(mesh):
    in_specs = (
        P("ep", None),
        P("ep", None),
        P("ep"),
        P("ep", None, "tp", None),
        P("ep", None, "tp", None),
        P(),
        P(None, "tp"),
        P("tp", None),
        P("tp"),
        P(),
        P(),
        P(),
        P("ep", None, "tp"),
        P("ep", None, "tp"),
        P("ep", "tp", None),
    )
    out_specs = P("ep", "tp")
    return jax.shard_map(
        per_device, mesh=mesh, in_specs=in_specs, out_specs=out_specs, check_vma=False
    )
```

profile of v0, /device:TPU:0, one launch (start us, length us, event | category | flops | bytes accessed | tf_op | source)
XLA Modules:
  0.0 132.4 jit_solution(12256758625774551817)
XLA Ops:
  6.5 1.2 fusion.28
  7.7 2.2 %convolution_convert_fusion.3 = bf16[32,512]{1,0:T(8,128)(2,1)S(1)} fusion(bf16[2048,512]{1,0:T(8,128)(2,1)} %param.21, bf16[32,2048]{1,0:T(8,128)(2,1)} %param.15, f32[2048]{0:T(1024)} %param.20, f32[32]{0:T(128)S(1)} %add_rsqrt_fusion.1), kind=kOutput, calls=%fused_computation.16 | convolution fusion | flops 67387392 | bytes 2269312 | tf_op jit(solution)/shard_map/dot_general | solution.py:59
  10.0 3.4 %fusion.37 = (f32[32,4,512]{2,1,0:T(4,128)S(1)}, f32[32,4,512]{2,1,0:T(4,128)S(1)}) fusion(s32[32]{0:T(128)} %param.17, f32[4]{0:T(128)} %param.23, bf16[32,4,128]{2,1,0:T(4,128)(2,1)S(1)} %reshape.157, bf16[32,512,1,128]{3,1,2,0:T(8,128)(2,1)} %param.18), kind=kOutput, calls=%fused_computation.41 | convolution fusion | flops 17498112 | bytes 4751504 | tf_op jit(solution)/shard_map/tkgd,tlkd->tkgl/dot_general | solution.py:23
  13.4 0.2 reshape.159
  13.7 19.9 %reduce-window.6 = f32[32,1,4,4,128]{4,0,2,1,3:T(8,128)S(1)} reduce-window(f32[32,1,4,4,128]{4,0,2,1,3:T(8,128)S(1)} %copy.41, f32[]{:T(128)} %constant.45.clone.1), window={size=1x1x1x1x128 pad=0_0x0_0x0_0x0_0x0_127}, to_apply=%region_1.2 | reduce-window | flops 8323072 | bytes 524292 | tf_op jit(solution)/shard_map/reduce-window
  33.6 0.2 copy.42
  33.8 0.2 copy.43
  34.0 0.1 copy.44
  34.1 0.2 broadcast.61
  34.3 0.2 reshape.163
  34.5 0.2 reshape.160
  34.7 3.2 %fusion.14 = bf16[32,4,128]{2,1,0:T(4,128)(2,1)S(1)} fusion(bf16[32,512,1,128]{3,1,2,0:T(8,128)(2,1)} %param.19, f32[32,4,512]{2,1,0:T(4,128)S(1)} %reshape.160, f32[32,4,512]{2,1,0:T(4,128)S(1)} %reshape.163, f32[32,4,512]{2,1,0:T(4,128)S(1)} %get-tuple-element.8, s32[32]{0:T(128)S(1)} %copy-done.3), kind=kOutput, calls=%fused_computation.17 | convolution fusion | flops 18235392 | bytes 5013632 | tf_op jit(solution)/shard_map/tkgl,tlkd->tkgd/dot_general | solution.py:33
  37.9 1.1 convolution_convert_fusion.1
  39.4 0.2 reduce_window_sum.25
  39.6 0.2 select_reduce_fusion
  39.9 0.8 dynamic_slice.7
  40.8 20.8 %reduce-scatter.3.cloned.1.call-done = bf16[32,512]{1,0:T(8,128)(2,1)} async-done(((bf16[32,2048]{1,0:T(8,128)(2,1)}), bf16[32,512]{1,0:T(8,128)(2,1)}) %reduce-scatter.3.cloned.1.call-update) | async-done | bytes 32784 | tf_op jit(solution)/shard_map/reduce_scatter | solution.py:66
  61.6 0.9 fusion.49
  62.5 5.8 %psum.7 = f32[32]{0:T(128)S(1)} all-reduce(f32[32]{0:T(128)S(1)} %get-tuple-element.5), channel_id=1, replica_groups=mesh['ep'=8,'tp'=4] {'tp'}, use_global_device_ids=true, to_apply=%region_5.6 | all-reduce | flops 32 | bytes 256 | tf_op jit(solution)/shard_map/psum | solution.py:72
  68.3 0.2 convolution_convert_fusion.2
  68.6 12.8 %all_to_all.10 = bf16[8,16,512]{2,1,0:T(8,128)(2,1)S(1)} all-to-all(bf16[8,16,512]{2,1,0:T(8,128)(2,1)S(1)} %bitcast.105), channel_id=1, replica_groups=mesh['ep'=8,'tp'=4] {'ep'}, dimensions={0} | all-to-all | bytes 262144 | tf_op jit(solution)/shard_map/all_to_all | solution.py:101
  81.4 6.5 %all_gather.7 = bf16[8,16,2048]{2,1,0:T(8,128)(2,1)S(1)} all-gather(bf16[8,16,512]{2,1,0:T(8,128)(2,1)S(1)} %all_to_all.10), channel_id=1, replica_groups=mesh['ep'=8,'tp'=4] {'tp'}, dimensions={2}, use_global_device_ids=true | all-gather | bytes 655360 | tf_op jit(solution)/shard_map/all_gather | solution.py:102
  87.9 1.5 %convolution_bitcast_fusion.1 = f32[8,1,16,256]{3,2,0,1:T(8,128)S(1)} fusion(bf16[8,16,2048]{2,1,0:T(8,128)(2,1)S(1)} %all_gather.7, bf16[1,2048,256]{2,1,0:T(8,128)(2,1)} %param.27), kind=kOutput, calls=%fused_computation.11 | convolution fusion | flops 134217728 | bytes 1703936 | tf_op jit(solution)/shard_map/nxcd,xdf->nxcf/dot_general | solution.py:105
  89.4 3.1 %convolution_convert_fusion = bf16[8,16,2048]{2,1,0:T(8,128)(2,1)} fusion(bf16[1,256,2048]{2,1,0:T(8,128)(2,1)} %param.29, bf16[8,16,2048]{2,1,0:T(8,128)(2,1)S(1)} %all_gather.7, bf16[1,2048,256]{2,1,0:T(8,128)(2,1)} %param.28, f32[8,1,16,256]{3,2,0,1:T(8,128)S(1)} %convolution_bitcast_fusion.1), kind=kOutput, calls=%fused_computation.4 | convolution fusion | flops 268894208 | bytes 3276800 | tf_op jit(solution)/shard_map/nxcf,xfd->nxcd/dot_general | solution.py:108
  92.6 5.4 %all_gather.6 = bf16[32,2048]{1,0:T(8,128)(2,1)S(1)} all-gather(bf16[32,512]{1,0:T(8,128)(2,1)S(1)} %fusion.51), channel_id=1, replica_groups=mesh['ep'=8,'tp'=4] {'tp'}, dimensions={1}, use_global_device_ids=true | all-gather | bytes 163840 | tf_op jit(solution)/shard_map/all_gather | solution.py:76
  98.1 0.1 fusion.63
  98.3 0.2 fusion.22
  98.4 13.4 %reduce-scatter.5.cloned.1.call-done = bf16[8,16,512]{2,1,0:T(8,128)(2,1)} async-done(((bf16[8,16,2048]{2,1,0:T(8,128)(2,1)}), bf16[8,16,512]{2,1,0:T(8,128)(2,1)}) %reduce-scatter.5.cloned.1.call-update) | async-done | bytes 131088 | tf_op jit(solution)/shard_map/reduce_scatter | solution.py:115
  111.9 5.5 %all-to-all-start.1 = ((bf16[8,16,512]{2,1,0:T(8,128)(2,1)}), bf16[8,16,512]{2,1,0:T(8,128)(2,1)S(1)}, u32[]{:S(2)}, u32[]{:S(2)}) async-start(bf16[8,16,512]{2,1,0:T(8,128)(2,1)} %reduce-scatter.5.cloned.1.call-done), calls=%async_computation.3 | async-start | bytes 262144 | tf_op jit(solution)/shard_map/all_to_all | solution.py:118
  117.5 0.2 fusion.54
  117.7 7.0 %all-to-all-done.1 = bf16[8,16,512]{2,1,0:T(8,128)(2,1)S(1)} async-done(((bf16[8,16,512]{2,1,0:T(8,128)(2,1)}), bf16[8,16,512]{2,1,0:T(8,128)(2,1)S(1)}, u32[]{:S(2)}, u32[]{:S(2)}) %all-to-all-start.1) | async-done | bytes 131104 | tf_op jit(solution)/shard_map/all_to_all | solution.py:118
  124.7 0.8 fusion.13
  (34 shorter events, 1.2 us)
Async XLA Ops:
  6.5 31.3 %copy-start = (bf16[512,2048]{1,0:T(8,128)(2,1)S(1)}, bf16[512,2048]{1,0:T(8,128)(2,1)}, u32[]{:S(2)}) copy-start(bf16[512,2048]{1,0:T(8,128)(2,1)} %param.22) | copy-start | bytes 6291460
  6.5 55.1 %reduce-scatter.3.cloned.1.call-start = ((), (), s32[]{:S(2)}) async-start(), calls=%async_computation.4 | async-start | bytes 163840 | tf_op jit(solution)/shard_map/reduce_scatter | solution.py:66
  10.0 24.7 %copy-start.3 = (s32[32]{0:T(128)S(1)}, s32[32]{0:T(128)}, u32[]{:S(2)}) copy-start(s32[32]{0:T(128)} %param.17) | copy-start | bytes 388
  34.6 4.5 %copy-start.2 = (s32[32,4]{0,1:T(4,128)S(1)}, s32[32,4]{0,1:T(4,128)}, u32[]{:S(2)}) copy-start(s32[32,4]{0,1:T(4,128)} %param.16) | copy-start | bytes 1540
  39.0 59.1 %copy-start.1 = (bf16[2048,8]{0,1:T(8,128)(2,1)S(1)}, bf16[2048,8]{0,1:T(8,128)(2,1)}, u32[]{:S(2)}) copy-start(bf16[2048,8]{0,1:T(8,128)(2,1)} %param.26) | copy-start | bytes 98308
  39.0 59.3 %copy-start.4 = (bf16[2048,1]{0,1:T(2,128)(2,1)S(1)}, bf16[2048,1]{0,1:T(2,128)(2,1)}, u32[]{:S(2)}) copy-start(bf16[2048,1]{0,1:T(2,128)(2,1)} %param.25) | copy-start | bytes 12292
  39.0 72.8 %reduce-scatter.5.cloned.1.call-start = ((), (), s32[]{:S(2)}) async-start(), calls=%async_computation.5 | async-start | bytes 655360 | tf_op jit(solution)/shard_map/reduce_scatter | solution.py:115
  111.9 12.8 %all-to-all-start.1 = ((bf16[8,16,512]{2,1,0:T(8,128)(2,1)}), bf16[8,16,512]{2,1,0:T(8,128)(2,1)S(1)}, u32[]{:S(2)}, u32[]{:S(2)}) async-start(bf16[8,16,512]{2,1,0:T(8,128)(2,1)} %reduce-scatter.5.cloned.1.call-done), calls=%async_computation.3 | async-start | bytes 262144 | tf_op jit(solution)/shard_map/all_to_all | solution.py:118
Sparse Core Ops, SparseCore 0:
  39.1 22.4 reduce-scatter.2
  92.7 19.1 reduce-scatter.4
where the time goes:
time: 133 us; the launch traced here: 132 us
  waiting for transfers between devices  41.3 us (31%)
  blocking collectives  30.5 us (23%)
  other arithmetic  22.8 us (17%)
  matrix products  16.2 us (12%)
  between operations  13.6 us (10%)
  starting transfers between devices  5.54 us (4%)
  local copies, waits for them, and re-layouts  2.47 us (2%)
    reduce_scatter x1, waiting for transfers between devices, per_device(): lax.psum_scatter(head_part.astype(jnp.bfloat16), 'tp', scatter_dimension=...  20.8 us
    another operation x2, other arithmetic  20 us
    reduce_scatter x1, waiting for transfers between devices, per_device(): lax.psum_scatter(partial_value.astype(jnp.bfloat16), 'tp', scatter_dimens...  13.4 us
    all_to_all x1, blocking collectives, per_device(): lax.all_to_all(outgoing, 'ep', split_axis=0, concat_axis=0, tiled=True)  12.8 us
    all_to_all x1, waiting for transfers between devices, per_device(): lax.all_to_all(summed, 'ep', split_axis=0, concat_axis=0, tiled=True)  6.99 us
    all_gather x1, blocking collectives, per_device(): arrived = lax.all_gather(arrived, 'tp', axis=2, tiled=True)  6.49 us
    psum x1, blocking collectives, per_device(): squares = lax.psum(jnp.sum(mid_values * mid_values, axis=1), 'tp')  5.76 us
    all_to_all x1, starting transfers between devices, per_device(): lax.all_to_all(summed, 'ep', split_axis=0, concat_axis=0, tiled=True)  5.5 us
  transfers between devices with their start and end apart: 3, of which 3 were waited for; matrix products, arithmetic and copies ran while one was open for 2% of the time, Pallas kernels for 0%

commit v1 on v0

--- a/solution.py
+++ b/solution.py
@@ -69,7 +69,12 @@
     res_own = lax.dynamic_slice_in_dim(residual, own_start, own_width, 1)
     mid_own = (res_own.astype(jnp.float32) + attn_own.astype(jnp.float32)).astype(jnp.bfloat16)
     mid_values = mid_own.astype(jnp.float32)
-    squares = lax.psum(jnp.sum(mid_values * mid_values, axis=1), "tp")
+
+    def _turn_space(mine, mesh_name):
+        piece_next = lax.all_gather(mine, mesh_name).sum(axis=0)
+        return piece_next
+
+    squares = _turn_space(jnp.sum(mid_values * mid_values, axis=1), "tp")
     inverse = lax.rsqrt(squares / width + EPSILON)
     gain_own = lax.dynamic_slice_in_dim(moe_gain, own_start, own_width, 0)
     send_rows = (mid_values * inverse[:, None] * gain_own[None, :]).astype(jnp.bfloat16)

time: 133 us -> 133 us (level)
    psum x1 -> x0, blocking collectives: 5.76 us -> none  [per_device(): squares = lax.psum(jnp.sum(mid_values * mid_values, axis=1), 'tp')]
    unnamed x0 -> x1, blocking collectives: none -> 5.73 us
where the time goes in v1:
time: 133 us
  waiting for transfers between devices  40 us (30%)
  blocking collectives  30.4 us (23%)
  other arithmetic  22.9 us (17%)
  matrix products  16.2 us (12%)
  between operations  14.3 us (11%)
  starting transfers between devices  5.54 us (4%)
  local copies, waits for them, and re-layouts  3.39 us (3%)
    another operation x2, other arithmetic  20 us
    reduce_scatter x1, waiting for transfers between devices, per_device(): lax.psum_scatter(head_part.astype(jnp.bfloat16), 'tp', scatter_dimension=...  19.6 us
    reduce_scatter x1, waiting for transfers between devices, per_device(): lax.psum_scatter(partial_value.astype(jnp.bfloat16), 'tp', scatter_dimens...  13.4 us
    all_to_all x1, blocking collectives, per_device(): lax.all_to_all(outgoing, 'ep', split_axis=0, concat_axis=0, tiled=True)  12.8 us
    all_to_all x1, waiting for transfers between devices, per_device(): lax.all_to_all(summed, 'ep', split_axis=0, concat_axis=0, tiled=True)  6.99 us
    all_gather x1, blocking collectives, per_device(): arrived = lax.all_gather(arrived, 'tp', axis=2, tiled=True)  6.49 us
    unnamed x1, blocking collectives  5.73 us
    all_to_all x1, starting transfers between devices, per_device(): lax.all_to_all(summed, 'ep', split_axis=0, concat_axis=0, tiled=True)  5.5 us
  transfers between devices with their start and end apart: 3, of which 3 were waited for; matrix products, arithmetic and copies ran while one was open for 2% of the time, Pallas kernels for 0%

profile of v1, /device:TPU:0, one launch (start us, length us, event | category | flops | bytes accessed | tf_op | source)
XLA Modules:
  0.0 132.7 jit_solution(10757813296367577478)
XLA Ops:
  6.5 1.2 fusion.28
  7.7 2.2 %convolution_convert_fusion.3 = bf16[32,512]{1,0:T(8,128)(2,1)S(1)} fusion(bf16[2048,512]{1,0:T(8,128)(2,1)} %param.21, bf16[32,2048]{1,0:T(8,128)(2,1)} %param.15, f32[2048]{0:T(1024)} %param.20, f32[32]{0:T(128)S(1)} %add_rsqrt_fusion.1), kind=kOutput, calls=%fused_computation.16 | convolution fusion | flops 67387392 | bytes 2269312 | tf_op jit(solution)/shard_map/dot_general | solution.py:59
  10.0 3.4 %fusion.37 = (f32[32,4,512]{2,1,0:T(4,128)S(1)}, f32[32,4,512]{2,1,0:T(4,128)S(1)}) fusion(s32[32]{0:T(128)} %param.17, f32[4]{0:T(128)} %param.23, bf16[32,4,128]{2,1,0:T(4,128)(2,1)S(1)} %reshape.161, bf16[32,512,1,128]{3,1,2,0:T(8,128)(2,1)} %param.18), kind=kOutput, calls=%fused_computation.41 | convolution fusion | flops 17498112 | bytes 4751504 | tf_op jit(solution)/shard_map/tkgd,tlkd->tkgl/dot_general | solution.py:23
  13.4 0.2 reshape.163
  13.7 19.9 %reduce-window.6 = f32[32,1,4,4,128]{4,0,2,1,3:T(8,128)S(1)} reduce-window(f32[32,1,4,4,128]{4,0,2,1,3:T(8,128)S(1)} %copy.41, f32[]{:T(128)} %constant.45.clone.1), window={size=1x1x1x1x128 pad=0_0x0_0x0_0x0_0x0_127}, to_apply=%region_1.2 | reduce-window | flops 8323072 | bytes 524292 | tf_op jit(solution)/shard_map/reduce-window
  33.6 0.2 copy.42
  33.8 0.2 copy.43
  34.1 0.2 broadcast.68
  34.3 0.2 reshape.167
  34.5 0.2 reshape.164
  34.7 3.2 %fusion.14 = bf16[32,4,128]{2,1,0:T(4,128)(2,1)S(1)} fusion(bf16[32,512,1,128]{3,1,2,0:T(8,128)(2,1)} %param.19, f32[32,4,512]{2,1,0:T(4,128)S(1)} %reshape.164, f32[32,4,512]{2,1,0:T(4,128)S(1)} %reshape.167, f32[32,4,512]{2,1,0:T(4,128)S(1)} %get-tuple-element.8, s32[32]{0:T(128)S(1)} %copy-done.3), kind=kOutput, calls=%fused_computation.17 | convolution fusion | flops 18235392 | bytes 5013632 | tf_op jit(solution)/shard_map/tkgl,tlkd->tkgd/dot_general | solution.py:33
  37.9 1.1 convolution_convert_fusion.1
  39.4 0.2 reduce_window_sum.25
  39.6 0.2 select_reduce_fusion
  39.9 0.6 dynamic-slice
  41.2 0.8 dynamic_slice.7
  42.1 19.6 %reduce-scatter.3.cloned.1.call-done = bf16[32,512]{1,0:T(8,128)(2,1)} async-done(((bf16[32,2048]{1,0:T(8,128)(2,1)}), bf16[32,512]{1,0:T(8,128)(2,1)}) %reduce-scatter.3.cloned.1.call-update) | async-done | bytes 32784 | tf_op jit(solution)/shard_map/reduce_scatter | solution.py:66
  61.6 0.9 fusion.49
  62.5 0.2 dynamic-update-slice
  62.8 5.7 %all-reduce = f32[128]{0:T(128)S(1)} all-reduce(f32[128]{0:T(128)S(1)} %dynamic-update-slice), channel_id=2, replica_groups=mesh['ep'=8,'tp'=4] {'tp'}, use_global_device_ids=true, to_apply=%add | all-reduce | flops 128 | bytes 1024
  68.7 0.2 convolution_convert_fusion.2
  68.9 12.8 %all_to_all.10 = bf16[8,16,512]{2,1,0:T(8,128)(2,1)S(1)} all-to-all(bf16[8,16,512]{2,1,0:T(8,128)(2,1)S(1)} %bitcast.106), channel_id=1, replica_groups=mesh['ep'=8,'tp'=4] {'ep'}, dimensions={0} | all-to-all | bytes 262144 | tf_op jit(solution)/shard_map/all_to_all | solution.py:106
  81.7 6.5 %all_gather.15 = bf16[8,16,2048]{2,1,0:T(8,128)(2,1)S(1)} all-gather(bf16[8,16,512]{2,1,0:T(8,128)(2,1)S(1)} %all_to_all.10), channel_id=1, replica_groups=mesh['ep'=8,'tp'=4] {'tp'}, dimensions={2}, use_global_device_ids=true | all-gather | bytes 655360 | tf_op jit(solution)/shard_map/all_gather | solution.py:107
  88.2 1.5 %convolution_bitcast_fusion.1 = f32[8,1,16,256]{3,2,0,1:T(8,128)S(1)} fusion(bf16[8,16,2048]{2,1,0:T(8,128)(2,1)S(1)} %all_gather.15, bf16[1,2048,256]{2,1,0:T(8,128)(2,1)} %param.27), kind=kOutput, calls=%fused_computation.11 | convolution fusion | flops 134217728 | bytes 1703936 | tf_op jit(solution)/shard_map/nxcd,xdf->nxcf/dot_general | solution.py:110
  89.7 3.1 %convolution_convert_fusion = bf16[8,16,2048]{2,1,0:T(8,128)(2,1)} fusion(bf16[1,256,2048]{2,1,0:T(8,128)(2,1)} %param.29, bf16[8,16,2048]{2,1,0:T(8,128)(2,1)S(1)} %all_gather.15, bf16[1,2048,256]{2,1,0:T(8,128)(2,1)} %param.28, f32[8,1,16,256]{3,2,0,1:T(8,128)S(1)} %convolution_bitcast_fusion.1), kind=kOutput, calls=%fused_computation.4 | convolution fusion | flops 268894208 | bytes 3276800 | tf_op jit(solution)/shard_map/nxcf,xfd->nxcd/dot_general | solution.py:113
  93.0 5.4 %all_gather.14 = bf16[32,2048]{1,0:T(8,128)(2,1)S(1)} all-gather(bf16[32,512]{1,0:T(8,128)(2,1)S(1)} %fusion.51), channel_id=1, replica_groups=mesh['ep'=8,'tp'=4] {'tp'}, dimensions={1}, use_global_device_ids=true | all-gather | bytes 163840 | tf_op jit(solution)/shard_map/all_gather | solution.py:81
  98.6 0.2 fusion.22
  98.8 13.4 %reduce-scatter.5.cloned.1.call-done = bf16[8,16,512]{2,1,0:T(8,128)(2,1)} async-done(((bf16[8,16,2048]{2,1,0:T(8,128)(2,1)}), bf16[8,16,512]{2,1,0:T(8,128)(2,1)}) %reduce-scatter.5.cloned.1.call-update) | async-done | bytes 131088 | tf_op jit(solution)/shard_map/reduce_scatter | solution.py:120
  112.2 5.5 %all-to-all-start.1 = ((bf16[8,16,512]{2,1,0:T(8,128)(2,1)}), bf16[8,16,512]{2,1,0:T(8,128)(2,1)S(1)}, u32[]{:S(2)}, u32[]{:S(2)}) async-start(bf16[8,16,512]{2,1,0:T(8,128)(2,1)} %reduce-scatter.5.cloned.1.call-done), calls=%async_computation.3 | async-start | bytes 262144 | tf_op jit(solution)/shard_map/all_to_all | solution.py:123
  117.8 0.2 fusion.54
  118.1 7.0 %all-to-all-done.1 = bf16[8,16,512]{2,1,0:T(8,128)(2,1)S(1)} async-done(((bf16[8,16,512]{2,1,0:T(8,128)(2,1)}), bf16[8,16,512]{2,1,0:T(8,128)(2,1)S(1)}, u32[]{:S(2)}, u32[]{:S(2)}) %all-to-all-start.1) | async-done | bytes 131104 | tf_op jit(solution)/shard_map/all_to_all | solution.py:123
  125.0 0.8 fusion.13
  (41 shorter events, 1.5 us)
Async XLA Ops:
  6.5 31.4 %copy-start = (bf16[512,2048]{1,0:T(8,128)(2,1)S(1)}, bf16[512,2048]{1,0:T(8,128)(2,1)}, u32[]{:S(2)}) copy-start(bf16[512,2048]{1,0:T(8,128)(2,1)} %param.22) | copy-start | bytes 6291460
  6.5 55.1 %reduce-scatter.3.cloned.1.call-start = ((), (), s32[]{:S(2)}) async-start(), calls=%async_computation.4 | async-start | bytes 163840 | tf_op jit(solution)/shard_map/reduce_scatter | solution.py:66
  10.0 24.7 %copy-start.3 = (s32[32]{0:T(128)S(1)}, s32[32]{0:T(128)}, u32[]{:S(2)}) copy-start(s32[32]{0:T(128)} %param.17) | copy-start | bytes 388
  34.6 4.5 %copy-start.2 = (s32[32,4]{0,1:T(4,128)S(1)}, s32[32,4]{0,1:T(4,128)}, u32[]{:S(2)}) copy-start(s32[32,4]{0,1:T(4,128)} %param.16) | copy-start | bytes 1540
  34.7 5.3 %copy-start.5 = (u32[32]{0:T(128)S(1)}, u32[32]{0:T(128)}, u32[]{:S(2)}) copy-start(u32[32]{0:T(128)} %constant.63) | copy-start | bytes 388
  39.0 59.4 %copy-start.1 = (bf16[2048,8]{0,1:T(8,128)(2,1)S(1)}, bf16[2048,8]{0,1:T(8,128)(2,1)}, u32[]{:S(2)}) copy-start(bf16[2048,8]{0,1:T(8,128)(2,1)} %param.26) | copy-start | bytes 98308
  39.0 59.6 %copy-start.4 = (bf16[2048,1]{0,1:T(2,128)(2,1)S(1)}, bf16[2048,1]{0,1:T(2,128)(2,1)}, u32[]{:S(2)}) copy-start(bf16[2048,1]{0,1:T(2,128)(2,1)} %param.25) | copy-start | bytes 12292
  39.0 73.2 %reduce-scatter.5.cloned.1.call-start = ((), (), s32[]{:S(2)}) async-start(), calls=%async_computation.5 | async-start | bytes 655360 | tf_op jit(solution)/shard_map/reduce_scatter | solution.py:120
  112.2 12.8 %all-to-all-start.1 = ((bf16[8,16,512]{2,1,0:T(8,128)(2,1)}), bf16[8,16,512]{2,1,0:T(8,128)(2,1)S(1)}, u32[]{:S(2)}, u32[]{:S(2)}) async-start(bf16[8,16,512]{2,1,0:T(8,128)(2,1)} %reduce-scatter.5.cloned.1.call-done), calls=%async_computation.3 | async-start | bytes 262144 | tf_op jit(solution)/shard_map/all_to_all | solution.py:123
Sparse Core Ops, SparseCore 0:
  39.2 22.4 reduce-scatter.2
  93.0 19.1 reduce-scatter.4
